TPU v7x, 32 devices: a whole 2x2x4 slice. The times are simulated.
32 devices in a mesh: fs: 8 (over z, x), tp: 4 (over y, core).
Axes of the slice: x: 2, y: 2, z: 4, core: 2. Of those that a mesh axis runs over, the one named last changes fastest.
Arguments:
- inputs: bfloat16 [8192, 2048], P('fs'), may hold values from -6 to 6
- cotangents: bfloat16 [8192, 3, 1024], P('fs', None, 'tp'), may hold values from -0.06591797 to 0.06591797
- factors: bfloat16 [3, 2048, 256], P(None, 'fs'), may hold values from -13.810679 to 13.810679
- first_moment: float32 [3, 256, 1024], P(None, None, 'tp'), may hold values from -6 to 6
- second_moment: float32 [3, 256, 1024], P(None, None, 'tp'), may hold values from 0.05 to 1
- master: float32 [3, 2048, 1024], P(None, 'fs', 'tp'), may hold values from -0.125 to 0.125
Outputs:
- update_step: float32 [3, 2048, 1024], P(None, 'fs', 'tp')
- new_master: float32 [3, 2048, 1024], P(None, 'fs', 'tp')
- new_copy: bfloat16 [3, 2048, 1024], P(None, None, 'tp')
- new_first: float32 [3, 256, 1024], P(None, None, 'tp')
- new_second: float32 [3, 256, 1024], P(None, None, 'tp')
All inputs are finite; a program needn't handle non-finite values.
Results may differ from a plain program's by a relative error of at most 0.001.
Values may be sent and summed in bfloat16 or wider, within the bound.
A program may use at most 64 MiB of HBM per device.

v0:
```python
import jax
import jax.numpy as jnp
from jax import lax
from jax.sharding import PartitionSpec as P

D = 2048
MW = 1024


beta_first = 0.8
beta_second = 0.9
adam_eps = 1e-08
norm_eps = 1e-06
learning_rate = 0.005


def local(inputs, cotangents, factors, first_moment, second_moment, master):
    factor32 = factors.astype(jnp.float32)
    lowered = jnp.einsum(
        "tk,mkr->mtr",
        inputs,
        lax.all_gather(factors, "fs", axis=1, tiled=True),
        preferred_element_type=jnp.float32,
    )
    cot_wide = cotangents.astype(jnp.float32)
    partial_value = jnp.einsum("mtr,tmc->mrc", lowered, cot_wide, precision=lax.Precision.HIGHEST)
    projected = lax.psum(partial_value, "fs")
    new_first = beta_first * first_moment + (1.0 - beta_first) * projected
    new_second = beta_second * second_moment + (1.0 - beta_second) * projected * projected
    normed = new_first / (jnp.sqrt(new_second) + adam_eps)
    update = jnp.einsum("mdr,mrc->mdc", factor32, normed, precision=lax.Precision.HIGHEST)
    squares = lax.psum(jnp.sum(update * update, axis=(1, 2)), ("fs", "tp"))
    root_mean = jnp.sqrt(squares / (D * MW) + norm_eps)
    update_step = update / root_mean[:, None, None]
    new_master = master - learning_rate * update_step
    new_copy = lax.all_gather(new_master.astype(jnp.bfloat16), "fs", axis=1, tiled=True)
    return (update_step, new_master, new_copy, new_first, new_second)


def solution(mesh):
    placed = (
        P("fs", None),
        P("fs", None, "tp"),
        P(None, "fs", None),
        P(None, None, "tp"),
        P(None, None, "tp"),
        P(None, "fs", "tp"),
    )
    return jax.shard_map(
        local,
        mesh=mesh,
        in_specs=placed,
        out_specs=(
            P(None, "fs", "tp"),
            P(None, "fs", "tp"),
            P(None, None, "tp"),
            P(None, None, "tp"),
            P(None, None, "tp"),
        ),
        check_vma=False,
    )
```

profile of v0, /device:TPU:0, one launch (start us, length us, event | category | flops | bytes accessed | tf_op | source)
XLA Modules:
  0.0 275.3 jit_solution(5420966089030130023)
XLA Ops:
  7.2 0.0 copy-start
  7.2 0.0 all-gather.3.cloned.1.call-start
  7.2 0.7 all-gather.3.cloned.1.call-update
  7.9 0.0 all-reduce.2.cloned.1.call-start
  8.0 65.0 %all-gather.3.cloned.1.call-done = bf16[3,2048,256]{2,1,0:T(8,128)(2,1)} async-done(((bf16[3,256,256]{2,1,0:T(8,128)(2,1)}), bf16[3,2048,256]{2,1,0:T(8,128)(2,1)}) %all-gather.3.cloned.1.call-update) | async-done | bytes 3145744 | tf_op jit(solution)/shard_map/all_gather | solution.py:22
  72.9 6.2 %fusion = f32[3,256,1024]{2,1,0:T(8,128)S(1)} fusion(bf16[3,2048,256]{2,1,0:T(8,128)(2,1)} %all-gather.3.cloned.1.call-done, bf16[1024,2048]{1,0:T(8,128)(2,1)} %param.6), kind=kOutput, calls=%fused_computation | convolution fusion | flops 3221225472 | bytes 10485760 | tf_op jit(solution)/shard_map/tk,mkr->mtr/dot_general | solution.py:19
  79.2 0.0 copy-done
  79.2 0.0 copy-start.1
  79.2 2.5 fusion.10
  81.7 0.0 copy-start.4
  81.7 0.0 all-reduce.2.cloned.1.call-update
  81.7 0.0 all-gather.5.cloned.1.call-start
  81.7 0.0 copy-done.1
  81.8 0.3 copy.12
  82.0 73.5 %all-reduce.2.cloned.1.call-done = f32[3,256,256]{2,1,0:T(8,128)} async-done(((f32[3,256,256]{2,1,0:T(8,128)}), f32[3,256,256]{2,1,0:T(8,128)}) %all-reduce.2.cloned.1.call-update) | async-done | bytes 786448 | tf_op jit(solution)/shard_map/psum | solution.py:27
  155.6 1.8 fusion.2
  157.4 0.0 copy-start.2
  157.4 0.0 copy-start.3
  157.4 0.9 copy-done.2
  158.3 0.0 copy-done.4
  158.3 1.8 multiply_reduce_fusion
  160.1 0.0 copy-done.3
  160.1 39.4 %psum.15 = f32[3]{0:T(128)S(1)} all-reduce(f32[3]{0:T(128)S(1)} %get-tuple-element.15), channel_id=1, replica_groups=mesh['fs'=8,'tp'=4] {'fs','tp'}, use_global_device_ids=true, to_apply=%region_2.0 | all-reduce | flops 3 | bytes 24 | tf_op jit(solution)/shard_map/psum | solution.py:32
  199.6 2.4 fusion.9
  202.0 0.0 all-gather.5.cloned.1.call-update
  202.0 2.3 copy.14
  204.3 1.1 copy.13
  205.4 58.7 %all-gather.5.cloned.1.call-done = bf16[3,2048,256]{1,2,0:T(8,128)(2,1)} async-done(((bf16[3,256,256]{1,2,0:T(8,128)(2,1)}), bf16[3,2048,256]{1,2,0:T(8,128)(2,1)}) %all-gather.5.cloned.1.call-update) | async-done | bytes 3145744 | tf_op jit(solution)/shard_map/all_gather | solution.py:36
  264.2 4.6 %copy.15 = bf16[3,2048,256]{2,1,0:T(8,128)(2,1)} copy(bf16[3,2048,256]{1,2,0:T(8,128)(2,1)} %all-gather.5.cloned.1.call-done) | data formatting | bytes 6291456
  (1 shorter events, 0.0 us)
Async XLA Ops:
  7.2 72.0 %copy-start = (bf16[1024,3,256]{2,0,1:T(8,128)(2,1)S(1)}, bf16[1024,3,256]{2,0,1:T(8,128)(2,1)}, u32[]{:S(2)}) copy-start(bf16[1024,3,256]{2,0,1:T(8,128)(2,1)} %param.7) | copy-start | bytes 4718596
  7.2 65.8 %all-gather.3.cloned.1.call-start = ((), (), s32[]{:S(2)}) async-start(), calls=%async_computation | async-start | bytes 3538944 | tf_op jit(solution)/shard_map/all_gather | solution.py:22
  7.9 147.7 %all-reduce.2.cloned.1.call-start = ((), (), s32[]{:S(2)}) async-start(), calls=%async_computation.1 | async-start | bytes 1572864 | tf_op jit(solution)/shard_map/psum | solution.py:27
  79.2 2.6 copy-start.1
  81.7 76.6 %copy-start.4 = (bf16[3,256,256]{2,1,0:T(8,128)(2,1)S(1)}, bf16[3,256,256]{2,1,0:T(8,128)(2,1)}, u32[]{:S(2)}) copy-start(bf16[3,256,256]{2,1,0:T(8,128)(2,1)} %param.8) | copy-start | bytes 1179652
  81.7 182.5 %all-gather.5.cloned.1.call-start = ((), (), s32[]{:S(2)}) async-start(), calls=%async_computation.2 | async-start | bytes 3538944 | tf_op jit(solution)/shard_map/all_gather | solution.py:36
  157.4 0.9 copy-start.2
  157.4 2.7 copy-start.3
Sparse Core Ops, SparseCore 0:
  10.2 62.7 all-gather.2
  81.8 73.7 all-reduce.1
  202.1 62.0 all-gather.4
where the time goes:
time: 276 us; the launch traced here: 275 us
  waiting for transfers between devices  198 us (72%)
  blocking collectives  39.4 us (14%)
  between operations  13.8 us (5%)
  matrix products  10.5 us (4%)
  local copies, waits for them, and re-layouts  9.21 us (3%)
  other arithmetic  4.22 us (2%)
    psum x1, waiting for transfers between devices, local(): projected = lax.psum(partial_value, 'fs')  73.5 us
    all_gather x1, waiting for transfers between devices, local(): lax.all_gather(factors, 'fs', axis=1, tiled=True)  65 us
    all_gather x1, waiting for transfers between devices, local(): lax.all_gather(new_master.astype(jnp.bfloat16), 'fs', axis=1, tiled=True)  58.7 us
    psum x1, blocking collectives, local(): squares = lax.psum(jnp.sum(update * update, axis=(1, 2)), ('fs', 'tp'))  39.4 us
    unnamed x14, local copies, waits for them, and re-layouts  9.21 us
    dot_general x1, matrix products, local(): jnp.einsum('tk,mkr->mtr', inputs, lax.all_gather(factors, 'fs', axis=1, t...  6.22 us
  transfers between devices with their start and end apart: 3, of which 3 were waited for; matrix products, arithmetic and copies ran while one was open for 1% of the time, Pallas kernels for 0%

commit v1 on v0

v1 whole, which is shorter than its diff:
```python
import functools

import jax
import jax.numpy as jnp
from jax import lax
from jax.experimental import pallas as pl
from jax.experimental.pallas import tpu as pltpu
from jax.sharding import PartitionSpec as P

beta_first = 0.8
beta_second = 0.9
adam_eps = 1e-08
norm_eps = 1e-06
learning_rate = 0.005

F32 = jnp.float32
BF16 = jnp.bfloat16


def split2(value):
    high = value.astype(BF16)
    low = (value - high.astype(F32)).astype(BF16)
    return high, low


def kernel(n, tp, width, x_hbm, cot_hbm, fac_hbm, first_hbm, second_hbm, master_hbm,
           step_out, newm_out, copy_out, nf_out, ns_out,
           x, cot, fg, first, second, master, part, got_pair, half_buf, got_line, full,
           step_v, newm_v, copy_v, nf_v, ns_v, upd, sq_mine, sq_all,
           in_sem, out_sem, f_send, f_recv, pair_send, pair_recv, rs_send, rs_recv,
           ag_send, ag_recv, sq_send, sq_recv, c_send, c_recv):
    mats, rows, rank = fac_hbm.shape
    depth = n * rows
    lines = n // 2
    half_rows = rows // 2
    half_rank = rank // 2
    me = lax.axis_index("fs")
    mt = lax.axis_index("tp")
    side = lax.rem(me, 2)
    q = me // 2
    partner = me + 1 - 2 * side
    core = lax.rem(mt, 2)
    mate = mt + 1 - 2 * core

    def remote(src, dst, ssem, rsem, fs=None, t=None):
        return pltpu.make_async_remote_copy(
            src_ref=src, dst_ref=dst, send_sem=ssem, recv_sem=rsem,
            device_id={"fs": me if fs is None else fs, "tp": mt if t is None else t},
            device_id_type=pl.DeviceIdType.MESH)

    my_rows = pl.ds(pl.multiple_of(me * rows, rows), rows)
    load_f = pltpu.make_async_copy(fac_hbm, fg.at[:, my_rows, :], in_sem.at[0])
    load_f.start()
    load_x = pltpu.make_async_copy(x_hbm, x, in_sem.at[1])
    load_x.start()
    load_c = pltpu.make_async_copy(cot_hbm, cot, in_sem.at[2])
    load_c.start()
    load_rest = [pltpu.make_async_copy(a, b, in_sem.at[3 + i]) for i, (a, b) in enumerate(
        ((first_hbm, first), (second_hbm, second), (master_hbm, master)))]
    for copy in load_rest:
        copy.start()

    barrier = pltpu.get_barrier_semaphore()
    for other in range(lines):
        @pl.when(other != q)
        def _():
            pl.semaphore_signal(barrier, inc=1, device_id={"fs": 2 * other + side, "tp": mt},
                                device_id_type=pl.DeviceIdType.MESH)
    pl.semaphore_signal(barrier, inc=1, device_id={"fs": partner, "tp": mt},
                        device_id_type=pl.DeviceIdType.MESH)
    for off in range(1, tp):
        pl.semaphore_signal(barrier, inc=1, device_id={"fs": me, "tp": lax.rem(mt + off, tp)},
                            device_id_type=pl.DeviceIdType.MESH)
    pl.semaphore_wait(barrier, lines - 1 + 1 + tp - 1)
    load_f.wait()

    def f_piece(m, fs, which):
        start = pl.multiple_of(fs * rows + which * half_rows, half_rows)
        return fg.at[m, pl.ds(start, half_rows), :]

    def f_copy(m, fs, kind, which=None):
        ref = f_piece(m, fs, core if which is None else which)
        if kind == 0:
            target = dict(fs=me - 2)
        elif kind == 1:
            target = dict(fs=me + 2)
        elif kind == 2:
            target = dict(fs=partner)
        else:
            target = dict(t=mate)
        slot = (core if which is None else which)
        return remote(ref, ref, f_send.at[m, fs, kind], f_recv.at[m, fs, slot], **target)

    def line_forward(copy_of, m, extra):
        for dist in range(1, lines):
            @pl.when(q >= dist)
            def _():
                src = me - 2 * dist
                copy_of(m, src, 1).wait_recv()

                @pl.when(q < lines - 1)
                def _():
                    copy_of(m, src, 1).start()
                copy_of(m, src, 2).start()
                if extra:
                    copy_of(m, src, 3).start()

            @pl.when(q + dist < lines)
            def _():
                src = me + 2 * dist
                copy_of(m, src, 0).wait_recv()

                @pl.when(q > 0)
                def _():
                    copy_of(m, src, 0).start()
                copy_of(m, src, 2).start()
                if extra:
                    copy_of(m, src, 3).start()

    def own_sends(copy_of, m):
        @pl.when(q < lines - 1)
        def _():
            copy_of(m, me, 1).start()

        @pl.when(q > 0)
        def _():
            copy_of(m, me, 0).start()
        copy_of(m, me, 2).start()

    def pair_arrivals(copy_of, m, extra):
        order = [0]
        for dist in range(1, lines):
            order += [-dist, dist]
        for dist in order:
            @pl.when((q + dist >= 0) & (q + dist < lines))
            def _():
                src = partner + 2 * dist
                copy_of(m, src, 2).wait_recv()
                if extra:
                    copy_of(m, src, 3).start()

    def drain(copy_of, m, extra):
        for dist in range(-(lines - 1), lines):
            if dist == 0:
                @pl.when(q < lines - 1)
                def _():
                    copy_of(m, me, 1).wait_send()

                @pl.when(q > 0)
                def _():
                    copy_of(m, me, 0).wait_send()
                copy_of(m, me, 2).wait_send()
                if extra:
                    copy_of(m, partner, 3).wait_send()
                continue

            @pl.when((q + dist >= 0) & (q + dist < lines))
            def _():
                src = me + 2 * dist
                if dist < 0:
                    @pl.when(q < lines - 1)
                    def _():
                        copy_of(m, src, 1).wait_send()
                else:
                    @pl.when(q > 0)
                    def _():
                        copy_of(m, src, 0).wait_send()
                copy_of(m, src, 2).wait_send()
                if extra:
                    copy_of(m, src, 3).wait_send()
                    copy_of(m, partner + 2 * dist, 3).wait_send()

    def mate_arrivals(m):
        for dist in range(1, n):
            src = lax.rem(me + dist, n)
            f_copy(m, src, 3, 1 - core).wait_recv()

    def f_gather(m):
        line_forward(f_copy, m, True)
        pair_arrivals(f_copy, m, True)
        mate_arrivals(m)

    def partial_of(m):
        lowered = jnp.dot(x[...], fg[m], preferred_element_type=F32)
        high, low = split2(lowered)
        c = cot[:, m, :]
        dims = (((0,), (0,)), ((), ()))
        value = lax.dot_general(high, c, dims, preferred_element_type=F32)
        value = value + lax.dot_general(low, c, dims, preferred_element_type=F32)
        part[m, 0] = value[:half_rank]
        part[m, 1] = value[half_rank:]

    def pair_copy(m):
        return remote(part.at[m, 1 - side], got_pair.at[m], pair_send.at[m], pair_recv.at[m], fs=partner)

    def rs_copy(m, other, slot):
        return remote(half_buf.at[m, other], got_line.at[m, slot], rs_send.at[m, other],
                      rs_recv.at[m, slot], fs=2 * other + side)

    def ag_copy(m, other, slot):
        ref = full.at[m, side, slot]
        return remote(ref, ref, ag_send.at[m, other], ag_recv.at[m, side, slot], fs=2 * other + side)

    def ag_pair(m, slot, arriving=False):
        s = 1 - side if arriving else side
        ref = full.at[m, s, slot]
        return remote(ref, ref, ag_send.at[m, lines + slot], ag_recv.at[m, s, slot], fs=partner)

    piece = half_rank // lines

    def rs_line(m):
        pair_copy(m).wait_recv()
        total = part[m, side] + got_pair[m]
        for j in range(lines):
            half_buf[m, j] = total[j * piece:(j + 1) * piece]
        for off in range(1, lines):
            other = lax.rem(q + off, lines)
            rs_copy(m, other, q).start()

    def rs_end(m):
        total = half_buf[m, q]
        for off in range(1, lines):
            src = lax.rem(q + off, lines)
            rs_copy(m, q, src).wait_recv()
            total = total + got_line[m, src]
        full[m, side, q] = total
        for off in range(1, lines):
            other = lax.rem(q + off, lines)
            ag_copy(m, other, q).start()
        ag_pair(m, q).start()

    def ag_forward(m):
        for off in range(1, lines):
            src = lax.rem(q + off, lines)
            ag_copy(m, q, src).wait_recv()
            ag_pair(m, src).start()

    def finish(m):
        for off in range(lines):
            ag_pair(m, lax.rem(q + off, lines), True).wait_recv()
        if m == 0:
            for copy in load_rest:
                copy.wait()
        projected = jnp.concatenate(
            [full[m, s, j] for s in range(2) for j in range(lines)], axis=0)
        nf = beta_first * first[m] + (1.0 - beta_first) * projected
        ns = beta_second * second[m] + (1.0 - beta_second) * projected * projected
        nf_v[m] = nf
        ns_v[m] = ns
        normed = nf / (jnp.sqrt(ns) + adam_eps)
        high, low = split2(normed)
        upd[m] = (jnp.dot(fg[m], high, preferred_element_type=F32)
                  + jnp.dot(fg[m], low, preferred_element_type=F32))
        value = upd[m]
        squares = jnp.sum(value * value)
        sq_mine[m] = jnp.full(sq_mine.shape[1:], squares, F32)
        sq_all[m, mt] = jnp.full(sq_mine.shape[1:], squares, F32)
        for off in range(1, tp):
            sq_copy(m, lax.rem(mt + off, tp), mt).start()
        pltpu.make_async_copy(nf_v.at[m], nf_out.at[m], out_sem.at[0, m]).start()
        pltpu.make_async_copy(ns_v.at[m], ns_out.at[m], out_sem.at[1, m]).start()

    def sq_copy(m, other, slot):
        return remote(sq_mine.at[m], sq_all.at[m, slot], sq_send.at[m, other], sq_recv.at[m, slot], t=other)

    def c_copy(m, fs, kind):
        ref = copy_v.at[m, pl.ds(pl.multiple_of(fs * rows, rows), rows), :]
        target = (me - 2, me + 2, partner)[kind]
        return remote(ref, ref, c_send.at[m, fs, kind], c_recv.at[m, fs], fs=target)

    def scale(m):
        for off in range(1, tp):
            src = lax.rem(mt + off, tp)
            sq_copy(m, mt, src).wait_recv()
        total = sq_all[m, 0]
        for t in range(1, tp):
            total = total + sq_all[m, t]
        root = jnp.sqrt(total[0:1, 0:1] / (depth * width) + norm_eps)
        step = upd[m, my_rows, :] / root
        new = master[m] - learning_rate * step
        copy_v[m, my_rows, :] = new.astype(BF16)
        own_sends(c_copy, m)
        step_v[m] = step
        newm_v[m] = new
        pltpu.make_async_copy(step_v.at[m], step_out.at[m], out_sem.at[2, m]).start()
        pltpu.make_async_copy(newm_v.at[m], newm_out.at[m], out_sem.at[3, m]).start()

    def copy_end(m):
        pair_arrivals(c_copy, m, False)
        pltpu.make_async_copy(copy_v.at[m], copy_out.at[m], out_sem.at[4, m]).start()

    for m in range(mats):
        own_sends(f_copy, m)
    for t in range(mats + 8):
        def at(stage, func):
            m = t - stage
            if 0 <= m < mats:
                func(m)
        at(0, f_gather)
        if t == 0:
            load_x.wait()
            load_c.wait()
        at(0, partial_of)
        at(0, lambda m: pair_copy(m).start())
        at(2, rs_end)
        at(1, rs_line)
        at(3, ag_forward)
        at(3, finish)
        at(4, scale)
        at(5, lambda m: line_forward(c_copy, m, False))
        at(6, copy_end)

    for m in range(mats):
        drain(f_copy, m, True)
        pair_copy(m).wait_send()
        for off in range(1, lines):
            other = lax.rem(q + off, lines)
            rs_copy(m, other, q).wait_send()
            ag_copy(m, other, q).wait_send()
        for slot in range(lines):
            ag_pair(m, slot).wait_send()
        for off in range(1, tp):
            sq_copy(m, lax.rem(mt + off, tp), mt).wait_send()
        drain(c_copy, m, False)
        for i, (a, b) in enumerate(((nf_v, nf_out), (ns_v, ns_out), (step_v, step_out), (newm_v, newm_out), (copy_v, copy_out))):
            pltpu.make_async_copy(a.at[m], b.at[m], out_sem.at[i, m]).wait()


def local(n, tp, inputs, cotangents, factors, first_moment, second_moment, master):
    tokens, depth = inputs.shape
    mats, rows, rank = factors.shape
    cols = cotangents.shape[2]
    lines = n // 2
    piece = rank // 2 // lines
    V = pltpu.VMEM
    dma = pltpu.SemaphoreType.DMA
    anyspec = pl.BlockSpec(memory_space=pl.ANY)
    small = jax.ShapeDtypeStruct((mats, rank, cols), F32)
    shard = jax.ShapeDtypeStruct((mats, rows, cols), F32)
    return pl.pallas_call(
        functools.partial(kernel, n, tp, cols * tp),
        out_shape=(shard, shard, jax.ShapeDtypeStruct((mats, depth, cols), BF16), small, small),
        in_specs=[anyspec] * 6,
        out_specs=(anyspec,) * 5,
        scratch_shapes=[
            V(inputs.shape, BF16), V(cotangents.shape, BF16), V((mats, depth, rank), BF16),
            V(small.shape, F32), V(small.shape, F32), V(shard.shape, F32),
            V((mats, 2, rank // 2, cols), F32), V((mats, rank // 2, cols), F32),
            V((mats, lines, piece, cols), F32), V((mats, lines, piece, cols), F32),
            V((mats, 2, lines, piece, cols), F32),
            V(shard.shape, F32), V(shard.shape, F32), V((mats, depth, cols), BF16),
            V(small.shape, F32), V(small.shape, F32), V((mats, depth, cols), F32),
            V((mats, 8, 128), F32), V((mats, tp, 8, 128), F32),
            dma((6,)), dma((5, mats)), dma((mats, n, 4)), dma((mats, n, 2)),
            dma((mats,)), dma((mats,)), dma((mats, lines)), dma((mats, lines)),
            dma((mats, 2 * lines)), dma((mats, 2, lines)), dma((mats, tp)), dma((mats, tp)),
            dma((mats, n, 3)), dma((mats, n)),
        ],
        compiler_params=pltpu.CompilerParams(
            collective_id=0, has_side_effects=True, vmem_limit_bytes=60 * 2 ** 20),
    )(inputs, cotangents, factors, first_moment, second_moment, master)


def solution(mesh):
    placed = (
        P("fs", None),
        P("fs", None, "tp"),
        P(None, "fs", None),
        P(None, None, "tp"),
        P(None, None, "tp"),
        P(None, "fs", "tp"),
    )
    return jax.shard_map(
        functools.partial(local, mesh.shape["fs"], mesh.shape["tp"]),
        mesh=mesh,
        in_specs=placed,
        out_specs=(
            P(None, "fs", "tp"),
            P(None, "fs", "tp"),
            P(None, None, "tp"),
            P(None, None, "tp"),
            P(None, None, "tp"),
        ),
        check_vma=False,
    )
```

time: 276 us -> 124 us (0.45)
  waiting for transfers between devices: 198 us -> 0 us
  Pallas kernels: 0 us -> 112 us
  blocking collectives: 39.4 us -> 0 us
  between operations: 13.8 us -> 0.65 us
  matrix products: 10.5 us -> 0 us
  other arithmetic: 4.22 us -> 0 us
    all_gather x2 -> x0, waiting for transfers between devices: 124 us -> none  [the longest x1 65 us: local(): lax.all_gather(factors, 'fs', axis=1, tiled=True)]
    pallas_call x0 -> x1, Pallas kernels: none -> 112 us  [local(): pl.pallas_call(functools.partial(kernel, n, tp, cols * tp), out_shape=(sh...]
    psum x1 -> x0, waiting for transfers between devices: 73.5 us -> none  [local(): projected = lax.psum(partial_value, 'fs')]
    psum x1 -> x0, blocking collectives: 39.4 us -> none  [local(): squares = lax.psum(jnp.sum(update * update, axis=(1, 2)), ('fs', 'tp'))]
    dot_general x3 -> x0, matrix products: 10.5 us -> none  [the longest x1 6.22 us: local(): jnp.einsum('tk,mkr->mtr', inputs, lax.all_gather(factors, 'fs', axis=1, t...]
    unnamed x14 -> x12, local copies, waits for them, and re-layouts: 9.21 us -> 11.8 us
  transfers between devices with their start and end apart: 3 -> 0, of which waited for: 3 -> 0; matrix products, arithmetic and copies ran while one was open for 1% -> 0% of each run, Pallas kernels for 0% -> 0%
where the time goes in v1:
time: 124 us
  Pallas kernels  112 us (90%)
  local copies, waits for them, and re-layouts  11.8 us (10%)
    pallas_call x1, Pallas kernels, local(): pl.pallas_call(functools.partial(kernel, n, tp, cols * tp), out_shape=(sh...  112 us
    unnamed x12, local copies, waits for them, and re-layouts  11.8 us

profile of v1, /device:TPU:0, one launch (start us, length us, event | category | flops | bytes accessed | tf_op | source)
XLA Modules:
  0.0 124.2 jit_solution(8436931998216672882)
XLA Ops:
  0.6 4.1 %copy.11.cot_hbm = bf16[1024,3,256]{2,1,0:T(4,128)(2,1)} copy(bf16[1024,3,256]{2,0,1:T(8,128)(2,1)} %param.7) | data formatting | bytes 3145728 | tf_op args[1]
  4.7 111.8 %shard_map.101 = (f32[3,256,256]{2,1,0:T(8,128)}, f32[3,256,256]{2,1,0:T(8,128)}, bf16[3,2048,256]{2,1,0:T(8,128)(2,1)}, f32[3,256,256]{2,1,0:T(8,128)}, f32[3,256,256]{2,1,0:T(8,128)}) custom-call(bf16[1024,2048]{1,0:T(8,128)(2,1)} %x_hbm.1, bf16[1024,3,256]{2,1,0:T(4,128)(2,1)} %copy.11.cot_hbm, bf16[3,256,256]{2,1,0:T(8,128)(2,1)} %fac_hbm.1, ...), custom_call_target="tpu_custom_call" | custom-call | tf_op jit(solution)/shard_map/pallas_call | solution.py:340
  116.5 0.0 copy-start
  116.5 2.2 %copy.17 = f32[3,256,256]{2,1,0:T(8,128)} copy(f32[3,256,256]{2,1,0:T(8,128)} %get-tuple-element.10) | data formatting | bytes 1572864
  118.7 2.1 %copy.18 = f32[3,256,256]{2,1,0:T(8,128)} copy(f32[3,256,256]{2,1,0:T(8,128)} %get-tuple-element.11) | data formatting | bytes 1572864
  120.8 0.0 copy-done
  120.8 0.0 copy-start.2
  120.8 0.0 copy-start.1
  120.8 1.7 %copy.19 = bf16[3,2048,256]{2,1,0:T(8,128)(2,1)} copy(bf16[3,2048,256]{2,1,0:T(8,128)(2,1)S(1)} %copy-done) | data formatting | bytes 6291456
  122.5 0.0 copy-done.2
  122.5 0.9 copy.20
  123.4 0.0 copy-done.1
  123.4 0.9 copy.21
Async XLA Ops:
  116.5 4.3 %copy-start = (bf16[3,2048,256]{2,1,0:T(8,128)(2,1)S(1)}, bf16[3,2048,256]{2,1,0:T(8,128)(2,1)}, u32[]{:S(2)}) copy-start(bf16[3,2048,256]{2,1,0:T(8,128)(2,1)} %get-tuple-element.12) | copy-start | bytes 9437188
  120.8 1.7 %copy-start.2 = (f32[3,256,256]{2,1,0:T(8,128)S(1)}, f32[3,256,256]{2,1,0:T(8,128)}, u32[]{:S(2)}) copy-start(f32[3,256,256]{2,1,0:T(8,128)} %get-tuple-element.13) | copy-start | bytes 2359300
  120.8 2.6 %copy-start.1 = (f32[3,256,256]{2,1,0:T(8,128)S(1)}, f32[3,256,256]{2,1,0:T(8,128)}, u32[]{:S(2)}) copy-start(f32[3,256,256]{2,1,0:T(8,128)} %get-tuple-element.14) | copy-start | bytes 2359300

commit v2 on v1

--- a/solution.py
+++ b/solution.py
@@ -24,10 +24,10 @@
 
 
 def kernel(n, tp, width, x_hbm, cot_hbm, fac_hbm, first_hbm, second_hbm, master_hbm,
-           step_out, newm_out, copy_out, nf_out, ns_out,
+           step_v, newm_v, copy_v, nf_v, ns_v,
            x, cot, fg, first, second, master, part, got_pair, half_buf, got_line, full,
-           step_v, newm_v, copy_v, nf_v, ns_v, upd, sq_mine, sq_all,
-           in_sem, out_sem, f_send, f_recv, pair_send, pair_recv, rs_send, rs_recv,
+           upd, sq_mine, sq_all,
+           in_sem, f_send, f_recv, pair_send, pair_recv, rs_send, rs_recv,
            ag_send, ag_recv, sq_send, sq_recv, c_send, c_recv):
     mats, rows, rank = fac_hbm.shape
     depth = n * rows
@@ -183,7 +183,7 @@
     def partial_of(m):
         lowered = jnp.dot(x[...], fg[m], preferred_element_type=F32)
         high, low = split2(lowered)
-        c = cot[:, m, :]
+        c = cot[m]
         dims = (((0,), (0,)), ((), ()))
         value = lax.dot_general(high, c, dims, preferred_element_type=F32)
         value = value + lax.dot_general(low, c, dims, preferred_element_type=F32)
@@ -257,8 +257,6 @@
         sq_all[m, mt] = jnp.full(sq_mine.shape[1:], squares, F32)
         for off in range(1, tp):
             sq_copy(m, lax.rem(mt + off, tp), mt).start()
-        pltpu.make_async_copy(nf_v.at[m], nf_out.at[m], out_sem.at[0, m]).start()
-        pltpu.make_async_copy(ns_v.at[m], ns_out.at[m], out_sem.at[1, m]).start()
 
     def sq_copy(m, other, slot):
         return remote(sq_mine.at[m], sq_all.at[m, slot], sq_send.at[m, other], sq_recv.at[m, slot], t=other)
@@ -282,12 +280,9 @@
         own_sends(c_copy, m)
         step_v[m] = step
         newm_v[m] = new
-        pltpu.make_async_copy(step_v.at[m], step_out.at[m], out_sem.at[2, m]).start()
-        pltpu.make_async_copy(newm_v.at[m], newm_out.at[m], out_sem.at[3, m]).start()
 
     def copy_end(m):
         pair_arrivals(c_copy, m, False)
-        pltpu.make_async_copy(copy_v.at[m], copy_out.at[m], out_sem.at[4, m]).start()
 
     for m in range(mats):
         own_sends(f_copy, m)
@@ -304,9 +299,9 @@
         at(0, lambda m: pair_copy(m).start())
         at(2, rs_end)
         at(1, rs_line)
+        at(4, scale)
         at(3, ag_forward)
         at(3, finish)
-        at(4, scale)
         at(5, lambda m: line_forward(c_copy, m, False))
         at(6, copy_end)
 
@@ -322,8 +317,15 @@
         for off in range(1, tp):
             sq_copy(m, lax.rem(mt + off, tp), mt).wait_send()
         drain(c_copy, m, False)
-        for i, (a, b) in enumerate(((nf_v, nf_out), (ns_v, ns_out), (step_v, step_out), (newm_v, newm_out), (copy_v, copy_out))):
-            pltpu.make_async_copy(a.at[m], b.at[m], out_sem.at[i, m]).wait()
+
+
+def write_out(*refs):
+    sem = refs[10]
+    copies = [pltpu.make_async_copy(refs[i], refs[5 + i], sem.at[i]) for i in range(5)]
+    for copy in copies:
+        copy.start()
+    for copy in copies:
+        copy.wait()
 
 
 def local(n, tp, inputs, cotangents, factors, first_moment, second_moment, master):
@@ -334,31 +336,38 @@
     piece = rank // 2 // lines
     V = pltpu.VMEM
     dma = pltpu.SemaphoreType.DMA
-    anyspec = pl.BlockSpec(memory_space=pl.ANY)
+    anyspec = pl.BlockSpec(memory_space=pltpu.HBM)
     small = jax.ShapeDtypeStruct((mats, rank, cols), F32)
     shard = jax.ShapeDtypeStruct((mats, rows, cols), F32)
-    return pl.pallas_call(
+    held = pl.pallas_call(
         functools.partial(kernel, n, tp, cols * tp),
-        out_shape=(shard, shard, jax.ShapeDtypeStruct((mats, depth, cols), BF16), small, small),
+        out_shape=(V(shard.shape, F32), V(shard.shape, F32), V((mats, depth, cols), BF16),
+                   V(small.shape, F32), V(small.shape, F32)),
         in_specs=[anyspec] * 6,
-        out_specs=(anyspec,) * 5,
+        out_specs=(pl.BlockSpec(memory_space=V),) * 5,
         scratch_shapes=[
-            V(inputs.shape, BF16), V(cotangents.shape, BF16), V((mats, depth, rank), BF16),
+            V(inputs.shape, BF16), V((mats, tokens, cols), BF16), V((mats, depth, rank), BF16),
             V(small.shape, F32), V(small.shape, F32), V(shard.shape, F32),
             V((mats, 2, rank // 2, cols), F32), V((mats, rank // 2, cols), F32),
             V((mats, lines, piece, cols), F32), V((mats, lines, piece, cols), F32),
             V((mats, 2, lines, piece, cols), F32),
-            V(shard.shape, F32), V(shard.shape, F32), V((mats, depth, cols), BF16),
-            V(small.shape, F32), V(small.shape, F32), V((mats, depth, cols), F32),
+            V((mats, depth, cols), F32),
             V((mats, 8, 128), F32), V((mats, tp, 8, 128), F32),
-            dma((6,)), dma((5, mats)), dma((mats, n, 4)), dma((mats, n, 2)),
+            dma((6,)), dma((mats, n, 4)), dma((mats, n, 2)),
             dma((mats,)), dma((mats,)), dma((mats, lines)), dma((mats, lines)),
             dma((mats, 2 * lines)), dma((mats, 2, lines)), dma((mats, tp)), dma((mats, tp)),
             dma((mats, n, 3)), dma((mats, n)),
         ],
         compiler_params=pltpu.CompilerParams(
-            collective_id=0, has_side_effects=True, vmem_limit_bytes=60 * 2 ** 20),
-    )(inputs, cotangents, factors, first_moment, second_moment, master)
+            collective_id=0, has_side_effects=True, vmem_limit_bytes=36 * 2 ** 20),
+    )(inputs, jnp.transpose(cotangents, (1, 0, 2)), factors, first_moment, second_moment, master)
+    return pl.pallas_call(
+        write_out,
+        out_shape=(shard, shard, jax.ShapeDtypeStruct((mats, depth, cols), BF16), small, small),
+        in_specs=[pl.BlockSpec(memory_space=V)] * 5,
+        out_specs=(anyspec,) * 5,
+        scratch_shapes=[dma((5,))],
+    )(*held)
 
 
 def solution(mesh):

time: 124 us -> 136 us (1.097)
  Pallas kernels: 112 us -> 122 us
  local copies, waits for them, and re-layouts: 11.8 us -> 13.2 us
    pallas_call x1 -> x2, Pallas kernels: 112 us -> 122 us  [the longest x1 116 us: local(): pl.pallas_call(functools.partial(kernel, n, tp, cols * tp), out_shape=(V(...]
    unnamed x12 -> x22, local copies, waits for them, and re-layouts: 11.8 us -> 13.2 us
where the time goes in v2:
time: 136 us
  Pallas kernels  122 us (90%)
  local copies, waits for them, and re-layouts  13.2 us (10%)
    pallas_call x1, Pallas kernels, local(): pl.pallas_call(functools.partial(kernel, n, tp, cols * tp), out_shape=(V(...  116 us
    unnamed x22, local copies, waits for them, and re-layouts  13.2 us
    pallas_call x1, Pallas kernels, local(): pl.pallas_call(write_out, out_shape=(shard, shard, jax.ShapeDtypeStruct((...  5.48 us

profile of v2, /device:TPU:0, one launch (start us, length us, event | category | flops | bytes accessed | tf_op | source)
XLA Modules:
  0.0 135.8 jit_solution(16600241550651173110)
XLA Ops:
  0.6 0.0 copy-start
  0.6 2.2 %copy-done = bf16[1024,2048]{1,0:T(8,128)(2,1)S(1)} copy-done((bf16[1024,2048]{1,0:T(8,128)(2,1)S(1)}, bf16[1024,2048]{1,0:T(8,128)(2,1)}, u32[]{:S(2)}) %copy-start) | copy-done | bytes 4194328
  2.8 0.0 copy-start.2
  2.8 1.4 %copy-done.2 = bf16[1024,3,256]{2,0,1:T(8,128)(2,1)S(1)} copy-done((bf16[1024,3,256]{2,0,1:T(8,128)(2,1)S(1)}, bf16[1024,3,256]{2,0,1:T(8,128)(2,1)}, u32[]{:S(2)}) %copy-start.2) | copy-done | bytes 1572888
  4.2 0.0 copy-start.3
  4.2 1.1 copy-done.3
  5.4 0.0 copy-start.4
  5.4 1.1 copy-done.4
  6.5 0.0 copy-start.5
  6.5 1.1 copy-done.5
  7.6 0.0 copy-start.10
  7.6 1.0 copy-done.10
  8.6 116.5 %shard_map.101 = (f32[3,256,256]{2,1,0:T(8,128)S(1)}, f32[3,256,256]{2,1,0:T(8,128)S(1)}, bf16[3,2048,256]{2,1,0:T(8,128)(2,1)S(1)}, f32[3,256,256]{2,1,0:T(8,128)S(1)}, f32[3,256,256]{2,1,0:T(8,128)S(1)}) custom-call(bf16[1024,2048]{1,0:T(8,128)(2,1)S(1)} %copy-done, bf16[3,1024,256]{2,1,0:T(8,128)(2,1)S(1)} %bitcast.1, ...), custom_call_target="tpu_custom_call" | custom-call | tf_op jit(solution)/shard_map/pallas_call | solution.py:342
  125.1 0.0 copy-start.1
  125.1 1.6 %copy-done.1 = bf16[3,2048,256]{2,1,0:T(8,128)(2,1)} copy-done((bf16[3,2048,256]{2,1,0:T(8,128)(2,1)}, bf16[3,2048,256]{2,1,0:T(8,128)(2,1)S(1)}, u32[]{:S(2)}) %copy-start.1) | copy-done | bytes 3145752
  126.7 0.0 copy-start.6
  126.7 0.9 copy-done.6
  127.6 0.0 copy-start.7
  127.6 0.9 copy-done.7
  128.5 0.0 copy-start.8
  128.5 0.9 copy-done.8
  129.4 0.0 copy-start.9
  129.4 0.9 copy-done.9
  130.3 5.5 %shard_map.102 = (f32[3,256,256]{2,1,0:T(8,128)}, f32[3,256,256]{2,1,0:T(8,128)}, bf16[3,2048,256]{2,1,0:T(8,128)(2,1)}, f32[3,256,256]{2,1,0:T(8,128)}, f32[3,256,256]{2,1,0:T(8,128)}) custom-call(f32[3,256,256]{2,1,0:T(8,128)} %copy-done.6, f32[3,256,256]{2,1,0:T(8,128)} %copy-done.7, bf16[3,2048,256]{2,1,0:T(8,128)(2,1)} %copy-done.1, ...), custom_call_target="tpu_custom_call" | custom-call | tf_op jit(solution)/shard_map/pallas_call | solution.py:364
Async XLA Ops:
  0.6 2.2 %copy-start = (bf16[1024,2048]{1,0:T(8,128)(2,1)S(1)}, bf16[1024,2048]{1,0:T(8,128)(2,1)}, u32[]{:S(2)}) copy-start(bf16[1024,2048]{1,0:T(8,128)(2,1)} %x_hbm.1) | copy-start | bytes 12582916
  2.8 1.4 %copy-start.2 = (bf16[1024,3,256]{2,0,1:T(8,128)(2,1)S(1)}, bf16[1024,3,256]{2,0,1:T(8,128)(2,1)}, u32[]{:S(2)}) copy-start(bf16[1024,3,256]{2,0,1:T(8,128)(2,1)} %param.7) | copy-start | bytes 4718596
  4.2 1.1 copy-start.3
  5.4 1.1 copy-start.4
  6.5 1.1 copy-start.5
  7.6 1.0 copy-start.10
  125.1 1.6 %copy-start.1 = (bf16[3,2048,256]{2,1,0:T(8,128)(2,1)}, bf16[3,2048,256]{2,1,0:T(8,128)(2,1)S(1)}, u32[]{:S(2)}) copy-start(bf16[3,2048,256]{2,1,0:T(8,128)(2,1)S(1)} %get-tuple-element.12.refs_2_) | copy-start | bytes 9437188
  126.7 0.9 copy-start.6
  127.6 0.9 copy-start.7
  128.5 0.9 copy-start.8
  129.4 0.9 copy-start.9
